TPU v7x, 32 devices: a whole 2x2x4 slice. The times are simulated.
32 devices in a mesh: dp: 4 (over y, x), kv: 4 (over z), tp: 2 (over core).
Axes of the slice: x: 2, y: 2, z: 4, core: 2. Of those that a mesh axis runs over, the one named last changes fastest.
Arguments:
- tokens: bfloat16 [16, 4096], P('dp', ('kv', 'tp')), may hold values from -75 to 75, as said below
- attn_gain: bfloat16 [4096], P('kv'), may hold values from 0.099609375 to 1.8984375
- w_query: bfloat16 [4096, 2048], P('kv', 'tp'), may hold values from -0.09375 to 0.09375
- w_key: bfloat16 [4096, 256], P('kv', 'tp'), may hold values from -0.75 to 0.75
- w_value: bfloat16 [4096, 256], P('kv', 'tp'), may hold values from -0.09375 to 0.09375
- key_cache: bfloat16 [16, 8192, 2, 128], P('dp', 'kv', 'tp'), may hold values from -700 to 700
- value_cache: bfloat16 [16, 8192, 2, 128], P('dp', 'kv', 'tp'), may hold values from -6 to 6
- lam: float32 [16], P('tp'), may hold values from 0.3 to 0.8
- head_gain: bfloat16 [128], replicated, may hold values from 0.099609375 to 1.8984375
- w_out: bfloat16 [2048, 4096], P('tp', 'kv'), may hold values from -0.125 to 0.125
- ffn_gain: bfloat16 [4096], replicated, may hold values from 0.099609375 to 1.8984375
- w_up: bfloat16 [4096, 16384], P(None, ('dp', 'kv', 'tp')), may hold values from -0.09375 to 0.09375
- w_down: bfloat16 [16384, 4096], P(('dp', 'kv', 'tp')), may hold values from -0.09375 to 0.09375
Outputs:
- updated: bfloat16 [16, 4096], P('dp', ('kv', 'tp'))
Inputs may be any that keep to these rules, and one draw needn't show every extreme that they name: `tokens`: column scales differ across the width.
All inputs are finite; a program needn't handle non-finite values.
Results may differ from a plain program's by a relative error of at most 0.017.
Values may be sent and summed in bfloat16 or wider, within the bound.
A program may use at most 64 MiB of HBM per device.

v0:
```python
import jax
import jax.numpy as jnp
from jax import lax
from jax.sharding import PartitionSpec as P

D = 4096
HD = 64
VD = 128


EPS = 1e-06
THETA = 500000.0
OUT_SCALE = 0.8


def joined(shard, axis, combine):
    everything = jax.tree.map(
        lambda part, kind: lax.all_gather(part.astype(kind), axis),
        shard,
        (jnp.bfloat16, jnp.bfloat16, jnp.bfloat16),
    )

    def take(k):
        return jax.tree.map(lambda part, own: part[k].astype(own.dtype), everything, shard)

    return lax.fori_loop(
        1, lax.axis_size(axis), lambda k, so_far: combine(so_far, take(k)), take(0)
    )


def settle(value):
    return lax.optimization_barrier(value.astype(jnp.bfloat16)).astype(jnp.float32)


def rotate(value, position):
    half = value.shape[-1] // 2
    inverse = THETA ** (-jnp.arange(half, dtype=jnp.float32) * 2.0 / value.shape[-1])
    angle = position * inverse
    cosine = jnp.cos(angle)
    sine = jnp.sin(angle)
    first = value[..., :half]
    second = value[..., half:]
    return jnp.concatenate(
        [first * cosine - second * sine, second * cosine + first * sine], axis=-1
    )


def combine_partials(first, second):
    top_a, den_a, num_a = first
    top_b, den_b, num_b = second
    top = jnp.maximum(top_a, top_b)
    factor_a = jnp.exp(top_a - top)
    factor_b = jnp.exp(top_b - top)
    return (
        top,
        den_a * factor_a + den_b * factor_b,
        num_a * factor_a[..., None] + num_b * factor_b[..., None],
    )


def local(
    tokens,
    attn_gain,
    w_query,
    w_key,
    w_value,
    key_cache,
    value_cache,
    lam,
    head_gain,
    w_out,
    ffn_gain,
    w_up,
    w_down,
):
    f32 = jnp.float32
    bf = jnp.bfloat16
    rows, width = tokens.shape
    kv_count = lax.axis_size("kv")
    tp_count = lax.axis_size("tp")
    dp_count = lax.axis_size("dp")
    positions = key_cache.shape[1]
    kv_local = key_cache.shape[2]
    heads_local = lam.shape[0]
    group = heads_local // kv_local
    scale = HD ** (-0.5)
    slab = lax.all_gather(tokens, "tp", axis=1, tiled=True)
    slab_f = slab.astype(f32)
    scaled = (slab_f * attn_gain.astype(f32)).astype(bf)
    part_q = jnp.dot(scaled, w_query, preferred_element_type=f32)
    part_k = jnp.dot(scaled, w_key, preferred_element_type=f32)
    part_v = jnp.dot(scaled, w_value, preferred_element_type=f32)
    local_sq = jnp.sum(slab_f * slab_f, axis=-1, keepdims=True)
    part_q, part_k, part_v, total_sq = lax.psum((part_q, part_k, part_v, local_sq), "kv")
    inv_rms = lax.rsqrt(total_sq / D + EPS)
    position = jnp.asarray(positions * kv_count, f32)
    query = rotate((part_q * inv_rms).reshape(rows, kv_local, group, 2, HD), position).astype(bf)
    new_key = rotate((part_k * inv_rms).reshape(rows, kv_local, 2, HD), position).astype(bf)
    new_value = (part_v * inv_rms).astype(bf).reshape(rows, kv_local, VD)
    cached_keys = key_cache.reshape(rows, positions, kv_local, 2, HD)
    scores = (
        jnp.einsum("rkgmd,rpkmd->rkgmp", query, cached_keys, preferred_element_type=f32) * scale
    )
    local_top = jnp.max(scores, axis=-1)
    expo = jnp.exp(scores - local_top[..., None])
    local_den = jnp.sum(expo, axis=-1)
    local_num = jnp.einsum(
        "rkgmp,rpkv->rkgmv", expo.astype(bf), value_cache, preferred_element_type=f32
    )
    top, den, num = joined((local_top, local_den, local_num), "kv", combine_partials)
    own_score = jnp.einsum("rkgmd,rkmd->rkgm", query, new_key, preferred_element_type=f32) * scale
    final_top = jnp.maximum(top, own_score)
    carried = jnp.exp(top - final_top)
    own_weight = jnp.exp(own_score - final_top)
    den = den * carried + own_weight
    num = (
        num * carried[..., None]
        + settle(own_weight)[..., None] * new_value.astype(f32)[:, :, None, None, :]
    )
    lam_h = lam.reshape(kv_local, group)
    mix = (
        num[..., 0, :] / den[..., 0, None]
        - lam_h[None, :, :, None] * num[..., 1, :] / den[..., 1, None]
    )
    normed = (
        mix
        * lax.rsqrt(jnp.mean(mix * mix, axis=-1, keepdims=True) + EPS)
        * head_gain.astype(f32)
        * OUT_SCALE
    )
    attended = normed.astype(bf).reshape(rows, heads_local * VD)
    part_out = jnp.dot(attended, w_out, preferred_element_type=f32)
    branch = lax.psum_scatter(
        part_out.astype(jnp.bfloat16), "tp", scatter_dimension=1, tiled=True
    ).astype(jnp.float32)
    hidden = (tokens.astype(f32) + branch).astype(bf)
    everyone = lax.all_gather(hidden[None], ("dp", "kv", "tp"), axis=0, tiled=True)
    blocks = kv_count * tp_count
    grid = everyone.reshape(dp_count, blocks, rows, width).astype(f32)
    row_sq = jnp.sum(grid * grid, axis=(1, 3))
    inv_two = lax.rsqrt(row_sq / D + EPS)
    gains = ffn_gain.astype(f32).reshape(blocks, width)
    normed_two = (grid * inv_two[:, None, :, None] * gains[None, :, None, :]).astype(bf)
    upward = jnp.einsum(
        "acrd,cdf->arf",
        normed_two,
        w_up.reshape(blocks, width, w_up.shape[1]),
        preferred_element_type=f32,
    )
    act = jnp.square(jax.nn.relu(upward)).astype(bf)
    down = jnp.einsum(
        "arf,fcd->acrd",
        act,
        w_down.reshape(w_down.shape[0], blocks, width),
        preferred_element_type=f32,
    )
    term = down.reshape(dp_count * blocks * rows, width)
    mixed = lax.psum_scatter(term, ("dp", "kv", "tp"), scatter_dimension=0, tiled=True)
    return (lax.optimization_barrier(hidden).astype(f32) + mixed).astype(bf)


def solution(mesh):
    in_specs = (
        P("dp", ("kv", "tp")),
        P("kv"),
        P("kv", "tp"),
        P("kv", "tp"),
        P("kv", "tp"),
        P("dp", "kv", "tp", None),
        P("dp", "kv", "tp", None),
        P("tp"),
        P(),
        P("tp", "kv"),
        P(),
        P(None, ("dp", "kv", "tp")),
        P(("dp", "kv", "tp"), None),
    )
    out_specs = P("dp", ("kv", "tp"))
    return jax.shard_map(local, mesh=mesh, in_specs=in_specs, out_specs=out_specs, check_vma=False)
```

profile of v0, /device:TPU:0, one launch (start us, length us, event | category | flops | bytes accessed | tf_op | source)
XLA Modules:
  0.0 269.8 jit_solution(11153000888686022137)
XLA Ops:
  6.6 2.2 all_gather.20
  8.8 0.7 convert_element_type.215
  9.5 0.1 fusion.27
  9.6 2.0 fusion.56
  11.6 0.1 fusion.52
  11.8 0.2 fusion.54
  11.9 20.6 %all-reduce.1 = (f32[4,1024]{1,0:T(4,128)S(1)}, f32[4,1]{0,1:T(1,128)S(1)}, f32[4,128]{1,0:T(4,128)S(1)}, f32[4,128]{1,0:T(4,128)S(1)}) all-reduce(f32[4,1024]{1,0:T(4,128)S(1)} %fusion.56, f32[4,1]{0,1:T(1,128)S(1)} %bitcast.225, f32[4,128]{1,0:T(4,128)S(1)} %fusion.52, ...), channel_id=1, replica_groups=mesh['dp'=4,'kv'=4,'tp'=2] {'kv'}, use_global_device_ids=true, to_apply=%region_0.0 | all-reduce | flops 5124 | bytes 40992 | tf_op jit(solution)/shard_map/psum | solution.py:94
  32.5 0.1 broadcast_multiply_fusion
  32.6 0.1 reshape.345
  32.7 0.1 fusion.64
  32.8 4.0 %copy.80 = bf16[4,2048,1,128]{1,3,0,2:T(8,128)(2,1)} copy(bf16[4,2048,1,128]{3,1,2,0:T(8,128)(2,1)} %param.20) | data formatting | bytes 4194304 | tf_op args[5]
  36.8 2.1 fusion.65
  38.9 0.2 fusion.19
  39.2 0.4 fusion.14
  39.6 13.1 %all-gather.2 = bf16[16,8,2,128]{3,1,2,0:T(8,128)(2,1)S(1)} all-gather(bf16[4,8,2,128]{3,1,2,0:T(8,128)(2,1)S(1)} %fusion.14), channel_id=4, replica_groups=mesh['dp'=4,'kv'=4,'tp'=2] {'kv'}, dimensions={0}, use_global_device_ids=true | all-gather | bytes 81920 | tf_op jit(solution)/shard_map/all_gather | solution.py:18
  52.8 11.9 %all-gather.1 = bf16[16,8,2]{1,2,0:T(2,128)(2,1)S(1)} all-gather(bf16[4,8,2]{1,2,0:T(2,128)(2,1)S(1)} %fusion.19), channel_id=3, replica_groups=mesh['dp'=4,'kv'=4,'tp'=2] {'kv'}, dimensions={0}, use_global_device_ids=true | all-gather | bytes 640 | tf_op jit(solution)/shard_map/all_gather | solution.py:18
  64.8 11.9 %all-gather = bf16[16,8,2]{1,2,0:T(2,128)(2,1)S(1)} all-gather(bf16[4,8,2]{1,2,0:T(2,128)(2,1)S(1)} %convert_element_type.217), channel_id=2, replica_groups=mesh['dp'=4,'kv'=4,'tp'=2] {'kv'}, dimensions={0}, use_global_device_ids=true | all-gather | bytes 640 | tf_op jit(solution)/shard_map/all_gather | solution.py:18
  76.7 1.6 while.19
  76.8 0.1 copy.199
  76.9 0.1 copy.200
  77.0 0.2 fusion.78
  77.3 0.1 copy.199
  77.4 0.1 copy.200
  77.5 0.2 fusion.78
  77.8 0.1 copy.199
  77.9 0.1 copy.200
  78.0 0.2 fusion.78
  78.4 0.1 reshape.349
  78.5 0.1 fusion.47
  78.5 0.1 maximum_bitcast_fusion
  78.6 0.2 fusion.43
  78.9 0.1 copy.91
  79.0 0.1 copy.90
  79.0 0.1 multiply_add_fusion
  79.4 0.2 multiply_reduce_fusion
  79.7 2.0 convolution_convert_fusion
  81.7 0.9 copy.107
  82.7 6.4 %reduce-scatter.4.cloned.1.call-done = bf16[512,4]{1,0:T(8,128)(2,1)} async-done(((bf16[1024,4]{1,0:T(8,128)(2,1)}), bf16[512,4]{1,0:T(8,128)(2,1)}) %reduce-scatter.4.cloned.1.call-update) | async-done | bytes 4112
  89.1 1.0 copy.108
  90.1 42.2 %all-gather.4 = bf16[32,4,512]{2,1,0:T(4,128)(2,1)S(1)} all-gather(bf16[1,4,512]{2,1,0:T(4,128)(2,1)S(1)} %bitcast.223), channel_id=5, replica_groups=mesh['dp'=4,'kv'=4,'tp'=2] {'dp','kv','tp'}, dimensions={0}, use_global_device_ids=true | all-gather | bytes 135168 | tf_op jit(solution)/shard_map/all_gather | solution.py:137
  132.3 0.1 fusion.22
  132.5 0.1 copy.112
  132.6 0.1 copy.118
  132.7 0.1 fusion.21
  132.8 4.9 %fusion.10 = f32[4,8,4,512]{3,2,1,0:T(4,128)S(1)} fusion(bf16[64,8,8,512]{3,2,1,0:T(8,128)(2,1)} %bitcast.211, bf16[4,8,4,512]{3,2,1,0:T(4,128)(2,1)S(1)} %bitcast.214, bf16[8,512,512,1]{2,1,0,3:T(8,128)(2,1)} %bitcast.212), kind=kOutput, calls=%fused_computation.23 | convolution fusion | flops 134242304 | bytes 8781824 | tf_op jit(solution)/shard_map/arf,fcd->acrd/dot_general | solution.py:151
  137.7 0.8 reshape.352
  138.5 123.1 %all-reduce.4.cloned.1.call-done = f32[128,512]{1,0:T(8,128)} async-done(((f32[128,512]{1,0:T(8,128)}), f32[128,512]{1,0:T(8,128)}) %all-reduce.4.cloned.1.call-update) | async-done | bytes 262160
  261.7 1.3 fusion.37
  (61 shorter events, 0.9 us)
Async XLA Ops:
  6.5 32.6 %copy-start = (bf16[4,2048,1,128]{3,1,2,0:T(8,128)(2,1)S(1)}, bf16[4,2048,1,128]{3,1,2,0:T(8,128)(2,1)}, u32[]{:S(2)}) copy-start(bf16[4,2048,1,128]{3,1,2,0:T(8,128)(2,1)} %param.21) | copy-start | bytes 6291460
  6.5 5.1 %copy-start.1 = (bf16[1024,128]{1,0:T(8,128)(2,1)S(1)}, bf16[1024,128]{1,0:T(8,128)(2,1)}, u32[]{:S(2)}) copy-start(bf16[1024,128]{1,0:T(8,128)(2,1)} %param.19) | copy-start | bytes 786436
  6.5 5.2 %copy-start.2 = (bf16[1024,128]{1,0:T(8,128)(2,1)S(1)}, bf16[1024,128]{1,0:T(8,128)(2,1)}, u32[]{:S(2)}) copy-start(bf16[1024,128]{1,0:T(8,128)(2,1)} %param.18) | copy-start | bytes 786436
  6.5 82.6 %reduce-scatter.4.cloned.1.call-start = ((), (), s32[]{:S(2)}) async-start(), calls=%async_computation.1 | async-start | bytes 393216
  39.2 40.2 %copy-start.5 = (f32[8]{0:T(128)S(1)}, f32[8]{0:T(128)}, u32[]{:S(2)}) copy-start(f32[8]{0:T(128)} %param.22) | copy-start | bytes 100
  39.2 40.5 %copy-start.6 = (bf16[128]{0:T(256)(128)(2,1)S(1)}, bf16[128]{0:T(256)(128)(2,1)}, u32[]{:S(2)}) copy-start(bf16[128]{0:T(256)(128)(2,1)} %param.23) | copy-start | bytes 772
  76.7 6.0 %copy-start.4 = (bf16[4096]{0:T(1024)(128)(2,1)S(1)}, bf16[4096]{0:T(1024)(128)(2,1)}, u32[]{:S(2)}) copy-start(bf16[4096]{0:T(1024)(128)(2,1)} %param.25) | copy-start | bytes 24580
  78.3 11.8 %copy-start.3 = (bf16[4,512]{1,0:T(4,128)(2,1)S(1)}, bf16[4,512]{1,0:T(4,128)(2,1)}, u32[]{:S(2)}) copy-start(bf16[4,512]{1,0:T(4,128)(2,1)} %param.15) | copy-start | bytes 12292
  82.6 179.0 %all-reduce.4.cloned.1.call-start = ((), (), s32[]{:S(2)}) async-start(), calls=%async_computation.2 | async-start | bytes 524288
Sparse Core Ops, SparseCore 0:
  82.7 6.3 reduce-scatter.3
  138.7 122.9 all-reduce.3
where the time goes:
time: 270 us
  waiting for transfers between devices  130 us (48%)
  blocking collectives  102 us (38%)
  between operations  13.6 us (5%)
  matrix products  11.9 us (4%)
  local copies, waits for them, and re-layouts  8.44 us (3%)
  other arithmetic  4.21 us (2%)
    unnamed x4, waiting for transfers between devices  130 us
    all_gather x1, blocking collectives, local(): lax.all_gather(hidden[None], ('dp', 'kv', 'tp'), axis=0, tiled=True)  42.2 us
    all_gather x3, blocking collectives, joined(): lax.all_gather(part.astype(kind), axis)  37 us
    psum x1, blocking collectives, local(): lax.psum((part_q, part_k, part_v, local_sq), 'kv')  20.6 us
    unnamed x22, local copies, waits for them, and re-layouts  6.33 us
  transfers between devices with their start and end apart: 2, of which 2 were waited for; matrix products, arithmetic and copies ran while one was open for 0% of the time, Pallas kernels for 0%

commit v1 on v0

v1 whole, which is shorter than its diff:
```python
import functools

import jax
import jax.numpy as jnp
import numpy as np
from jax import lax
from jax.experimental import pallas as pl
from jax.experimental.pallas import tpu as pltpu
from jax.sharding import PartitionSpec as P

HD = 64
VD = 128

EPS = 1e-06
THETA = 500000.0
OUT_SCALE = 0.8
MESH = pl.DeviceIdType.MESH
F32 = jnp.float32
BF = jnp.bfloat16


def rope_table(position):
    half = HD // 2
    inverse = THETA ** (-np.arange(half, dtype=np.float64) * 2.0 / HD)
    angle = position * inverse
    cosine = np.tile(np.cos(angle), 4)
    sine = np.tile(np.concatenate([-np.sin(angle), np.sin(angle)]), 2)
    return np.stack([cosine, sine]).astype(np.float32)


def rotate(value, table):
    half = HD // 2
    lane = lax.broadcasted_iota(jnp.int32, value.shape, 1)
    swapped = jnp.where(
        lane % HD < half, pltpu.roll(value, VD - half, 1), pltpu.roll(value, half, 1)
    )
    return value * table[0:1, :] + swapped * table[1:2, :]


def kernel(
    dims,
    tok,
    gain,
    lam,
    head_gain,
    ffn_gain,
    table,
    wq,
    wk,
    wv,
    kc,
    vc,
    wo,
    wu,
    wd,
    out,
    wq_v,
    wk_v,
    wv_v,
    kc_v,
    vc_v,
    wo_v,
    wu_v,
    wd_v,
    slab,
    part,
    q_rows,
    k_rows,
    o_part,
    s_part,
    att,
    half_out,
    half_in,
    hid,
    grid,
    down_out,
    down_in,
    load_sem,
    slab_sem,
    part_sem,
    o_sem,
    s_sem,
    half_sem,
    hid_sem,
    down_sem,
):
    n_dp, n_kv, n_tp = dims
    n = n_dp * n_kv * n_tp
    blocks = n_kv * n_tp
    rows, width = tok.shape
    heads = lam.shape[0]
    q_cols = heads * VD
    model = blocks * width
    scale = HD ** (-0.5)
    i_dp, i_kv, i_tp = lax.axis_index("dp"), lax.axis_index("kv"), lax.axis_index("tp")
    me = (i_dp * n_kv + i_kv) * n_tp + i_tp

    def device(p):
        return (p // blocks, (p // n_tp) % n_kv, p % n_tp)

    loads = [
        pltpu.make_async_copy(src, dst, load_sem.at[k])
        for k, (src, dst) in enumerate(
            (
                (wq, wq_v),
                (wk, wk_v),
                (wv, wv_v),
                (kc, kc_v),
                (vc, vc_v),
                (wo, wo_v),
                (wu, wu_v),
                (wd, wd_v),
            )
        )
    ]
    for load in loads:
        load.start()

    barrier = pltpu.get_barrier_semaphore()

    def greet(i, carry):
        pl.semaphore_signal(
            barrier, inc=1, device_id=device((me + i) % n), device_id_type=MESH
        )
        return carry

    lax.fori_loop(1, n, greet, 0)
    pl.semaphore_wait(barrier, n - 1)

    def to_tp(i, src, dst, sem):
        peer = (i_tp + i) % n_tp
        return pltpu.make_async_remote_copy(
            src_ref=src(peer),
            dst_ref=dst.at[i_tp],
            send_sem=sem.at[0, peer],
            recv_sem=sem.at[1, i_tp],
            device_id=(i_dp, i_kv, peer),
            device_id_type=MESH,
        )

    def from_tp(i, dst, sem):
        peer = (i_tp + i) % n_tp
        return pltpu.make_async_remote_copy(
            src_ref=dst.at[peer],
            dst_ref=dst.at[peer],
            send_sem=sem.at[0, peer],
            recv_sem=sem.at[1, peer],
            device_id=(i_dp, i_kv, peer),
            device_id_type=MESH,
        )

    def to_kv(i, dst, sem):
        peer = (i_kv + i) % n_kv
        return pltpu.make_async_remote_copy(
            src_ref=dst.at[i_kv],
            dst_ref=dst.at[i_kv],
            send_sem=sem.at[0, peer],
            recv_sem=sem.at[1, i_kv],
            device_id=(i_dp, peer, i_tp),
            device_id_type=MESH,
        )

    def from_kv(i, dst, sem):
        peer = (i_kv + i) % n_kv
        return pltpu.make_async_remote_copy(
            src_ref=dst.at[peer],
            dst_ref=dst.at[peer],
            send_sem=sem.at[0, peer],
            recv_sem=sem.at[1, peer],
            device_id=(i_dp, peer, i_tp),
            device_id_type=MESH,
        )

    def to_all(i, src, dst, sem):
        peer = (me + i) % n
        return pltpu.make_async_remote_copy(
            src_ref=src(peer),
            dst_ref=dst.at[me],
            send_sem=sem.at[0, peer],
            recv_sem=sem.at[1, me],
            device_id=device(peer),
            device_id_type=MESH,
        )

    def from_all(i, dst, sem):
        peer = (me + i) % n
        return pltpu.make_async_remote_copy(
            src_ref=dst.at[peer],
            dst_ref=dst.at[peer],
            send_sem=sem.at[0, peer],
            recv_sem=sem.at[1, peer],
            device_id=device(peer),
            device_id_type=MESH,
        )

    def each(count, act):
        def step(i, carry):
            act(i)
            return carry

        lax.fori_loop(1, count, step, 0)

    for i in range(1, n_tp):
        to_tp(i, lambda peer: tok, slab, slab_sem).start()
    slab[i_tp] = tok[...]
    for load in loads[:3]:
        load.wait()
    for i in range(1, n_tp):
        from_tp(i, slab, slab_sem).wait_recv()

    part_q = jnp.zeros((rows, q_cols), F32)
    part_k = jnp.zeros((rows, VD), F32)
    part_v = jnp.zeros((rows, VD), F32)
    local_sq = jnp.zeros((rows, 1), F32)
    for t in range(n_tp):
        span = slice(t * width, (t + 1) * width)
        value = slab[t].astype(F32)
        local_sq += jnp.sum(value * value, axis=-1, keepdims=True)
        scaled = (value * gain[:, span].astype(F32)).astype(BF)
        part_q += jnp.dot(scaled, wq_v[span, :], preferred_element_type=F32)
        part_k += jnp.dot(scaled, wk_v[span, :], preferred_element_type=F32)
        part_v += jnp.dot(scaled, wv_v[span, :], preferred_element_type=F32)
    part[i_kv, :, 0:q_cols] = part_q
    part[i_kv, :, q_cols : q_cols + VD] = part_k
    part[i_kv, :, q_cols + VD : q_cols + 2 * VD] = part_v
    part[i_kv, :, q_cols + 2 * VD : q_cols + 3 * VD] = jnp.broadcast_to(local_sq, (rows, VD))
    each(n_kv, lambda i: to_kv(i, part, part_sem).start())
    each(n_kv, lambda i: from_kv(i, part, part_sem).wait_recv())

    total = part[0]
    for k in range(1, n_kv):
        total += part[k]
    inv_rms = lax.rsqrt(total[:, q_cols + 2 * VD : q_cols + 2 * VD + 1] / model + EPS)
    table_v = table[...]
    for h in range(heads):
        chunk = total[:, h * VD : (h + 1) * VD] * inv_rms
        for r in range(rows):
            q_rows[r, h : h + 1, :] = chunk[r : r + 1, :]
    k_rows[...] = jnp.zeros_like(k_rows)
    k_rows[0:rows, :] = total[:, q_cols : q_cols + VD] * inv_rms
    new_key = rotate(k_rows[...], table_v).astype(BF).astype(F32)
    new_value = (total[:, q_cols + VD : q_cols + 2 * VD] * inv_rms).astype(BF).astype(F32)

    for load in loads[3:5]:
        load.wait()
    pairs = 2 * heads
    lane_h = lax.broadcasted_iota(jnp.int32, (heads, VD), 1)
    lane_p = lax.broadcasted_iota(jnp.int32, (pairs, VD), 1)
    row_p = lax.broadcasted_iota(jnp.int32, (pairs, VD), 0)
    own_scores = []
    stat_row = jnp.zeros((1, VD), F32)
    for r in range(rows):
        query = rotate(q_rows[r], table_v).astype(BF).astype(F32)
        both = jnp.concatenate(
            [jnp.where(lane_h < HD, query, 0.0), jnp.where(lane_h < HD, 0.0, query)], axis=0
        )
        own_scores.append(
            jnp.sum(both * new_key[r : r + 1, :], axis=-1, keepdims=True) * scale
        )
        scores = (
            lax.dot_general(
                both.astype(BF), kc_v[r], (((1,), (1,)), ((), ())), preferred_element_type=F32
            )
            * scale
        )
        top = jnp.max(scores, axis=-1, keepdims=True)
        expo = jnp.exp(scores - top)
        den = jnp.sum(expo, axis=-1, keepdims=True)
        num = jnp.dot(expo.astype(BF), vc_v[r], preferred_element_type=F32)
        o_part[i_kv, r] = (num / den).astype(BF)
        stat = top + jnp.log(den)
        stat_row += jnp.sum(
            jnp.where(lane_p == row_p + r * pairs, stat, 0.0), axis=0, keepdims=True
        )
    s_part[i_kv] = jnp.broadcast_to(stat_row, (8, VD))
    each(n_kv, lambda i: to_kv(i, s_part, s_sem).start())
    each(n_kv, lambda i: to_kv(i, o_part, o_sem).start())
    each(n_kv, lambda i: from_kv(i, s_part, s_sem).wait_recv())
    each(n_kv, lambda i: from_kv(i, o_part, o_sem).wait_recv())

    lam_h = lam[...]
    for r in range(rows):
        own = own_scores[r]
        stats = []
        top = own
        for k in range(n_kv):
            stat = jnp.sum(
                jnp.where(lane_p == row_p + r * pairs, s_part[k][0:1, :], 0.0),
                axis=-1,
                keepdims=True,
            )
            stats.append(stat)
            top = jnp.maximum(top, stat)
        own_weight = jnp.exp(own - top)
        den = own_weight
        num = own_weight * new_value[r : r + 1, :]
        for k in range(n_kv):
            weight = jnp.exp(stats[k] - top)
            den += weight
            num += weight * o_part[k, r].astype(F32)
        ratio = num / den
        mix = ratio[0:heads, :] - lam_h * ratio[heads:, :]
        normed = (
            mix
            * lax.rsqrt(jnp.mean(mix * mix, axis=-1, keepdims=True) + EPS)
            * head_gain[...].astype(F32)
            * OUT_SCALE
        )
        for h in range(heads):
            att[r : r + 1, h * VD : (h + 1) * VD] = normed[h : h + 1, :]

    loads[5].wait()
    part_out = jnp.dot(att[...].astype(BF), wo_v[...], preferred_element_type=F32)
    for t in range(n_tp):
        half_out[t] = part_out[:, t * width : (t + 1) * width].astype(BF)
    for i in range(1, n_tp):
        to_tp(i, lambda peer: half_out.at[peer], half_in, half_sem).start()
    half_in[i_tp] = half_out[i_tp]
    for i in range(1, n_tp):
        from_tp(i, half_in, half_sem).wait_recv()
    branch = half_in[0].astype(F32)
    for t in range(1, n_tp):
        branch += half_in[t].astype(F32)
    hidden = (tok[...].astype(F32) + branch).astype(BF)
    hid[me] = hidden
    each(n, lambda i: to_all(i, lambda peer: hid.at[me], hid, hid_sem).start())
    each(n, lambda i: from_all(i, hid, hid_sem).wait_recv())

    row_sq = jnp.zeros((n_dp * rows, 1), F32)
    for c in range(blocks):
        for a in range(n_dp):
            grid[c, a * rows : (a + 1) * rows, :] = hid[a * blocks + c].astype(F32)
        value = grid[c]
        row_sq += jnp.sum(value * value, axis=-1, keepdims=True)
    inv_two = lax.rsqrt(row_sq / model + EPS)
    loads[6].wait()
    upward = jnp.zeros((n_dp * rows, wu_v.shape[1]), F32)
    for c in range(blocks):
        span = slice(c * width, (c + 1) * width)
        normed_two = (grid[c] * inv_two * ffn_gain[:, span].astype(F32)).astype(BF)
        upward += jnp.dot(normed_two, wu_v[span, :], preferred_element_type=F32)
    act = jnp.square(jnp.maximum(upward, 0.0)).astype(BF)
    loads[7].wait()
    for c in range(blocks):
        span = slice(c * width, (c + 1) * width)
        down = jnp.dot(act, wd_v[:, span], preferred_element_type=F32)
        for a in range(n_dp):
            down_out[a * blocks + c] = down[a * rows : (a + 1) * rows, :].astype(BF)
    each(n, lambda i: to_all(i, lambda peer: down_out.at[peer], down_in, down_sem).start())
    down_in[me] = down_out[me]
    each(n, lambda i: from_all(i, down_in, down_sem).wait_recv())
    mixed = down_in[0].astype(F32)
    for p in range(1, n):
        mixed += down_in[p].astype(F32)
    out[...] = (hidden.astype(F32) + mixed).astype(BF)

    for i in range(1, n_tp):
        to_tp(i, lambda peer: tok, slab, slab_sem).wait_send()
        to_tp(i, lambda peer: half_out.at[peer], half_in, half_sem).wait_send()
    for dst, sem in ((part, part_sem), (s_part, s_sem), (o_part, o_sem)):
        each(n_kv, lambda i: to_kv(i, dst, sem).wait_send())
    each(n, lambda i: to_all(i, lambda peer: hid.at[me], hid, hid_sem).wait_send())
    each(n, lambda i: to_all(i, lambda peer: down_out.at[peer], down_in, down_sem).wait_send())


def local(
    dims,
    tokens,
    attn_gain,
    w_query,
    w_key,
    w_value,
    key_cache,
    value_cache,
    lam,
    head_gain,
    w_out,
    ffn_gain,
    w_up,
    w_down,
):
    n_dp, n_kv, n_tp = dims
    n = n_dp * n_kv * n_tp
    blocks = n_kv * n_tp
    rows, width = tokens.shape
    positions = key_cache.shape[1]
    heads = lam.shape[0]
    keys = key_cache.reshape(rows, positions, VD)
    values = value_cache.reshape(rows, positions, VD)
    table = jnp.asarray(rope_table(positions * n_kv))
    vmem = pl.BlockSpec(memory_space=pltpu.VMEM)
    hbm = pl.BlockSpec(memory_space=pl.ANY)
    big = (w_query, w_key, w_value, keys, values, w_out, w_up, w_down)
    dma = pltpu.SemaphoreType.DMA
    return pl.pallas_call(
        functools.partial(kernel, dims),
        name="layer",
        out_shape=jax.ShapeDtypeStruct((rows, width), BF),
        in_specs=[vmem] * 6 + [hbm] * 8,
        out_specs=vmem,
        scratch_shapes=[pltpu.VMEM(a.shape, BF) for a in big]
        + [
            pltpu.VMEM((n_tp, rows, width), BF),
            pltpu.VMEM((n_kv, rows, heads * VD + 3 * VD), F32),
            pltpu.VMEM((rows, heads, VD), F32),
            pltpu.VMEM((8, VD), F32),
            pltpu.VMEM((n_kv, rows, 2 * heads, VD), BF),
            pltpu.VMEM((n_kv, 8, VD), F32),
            pltpu.VMEM((rows, heads * VD), F32),
            pltpu.VMEM((n_tp, rows, width), BF),
            pltpu.VMEM((n_tp, rows, width), BF),
            pltpu.VMEM((n, rows, width), BF),
            pltpu.VMEM((blocks, n_dp * rows, width), F32),
            pltpu.VMEM((n, rows, width), BF),
            pltpu.VMEM((n, rows, width), BF),
            dma((8,)),
            dma((2, n_tp)),
            dma((2, n_kv)),
            dma((2, n_kv)),
            dma((2, n_kv)),
            dma((2, n_tp)),
            dma((2, n)),
            dma((2, n)),
        ],
        compiler_params=pltpu.CompilerParams(
            collective_id=0, has_side_effects=True, vmem_limit_bytes=60 * 1024 * 1024
        ),
    )(
        tokens,
        attn_gain.reshape(1, -1),
        lam.reshape(-1, 1),
        head_gain.reshape(1, -1),
        ffn_gain.reshape(1, -1),
        table,
        *big,
    )


def solution(mesh):
    in_specs = (
        P("dp", ("kv", "tp")),
        P("kv"),
        P("kv", "tp"),
        P("kv", "tp"),
        P("kv", "tp"),
        P("dp", "kv", "tp", None),
        P("dp", "kv", "tp", None),
        P("tp"),
        P(),
        P("tp", "kv"),
        P(),
        P(None, ("dp", "kv", "tp")),
        P(("dp", "kv", "tp"), None),
    )
    out_specs = P("dp", ("kv", "tp"))
    dims = (mesh.shape["dp"], mesh.shape["kv"], mesh.shape["tp"])
    return jax.shard_map(
        functools.partial(local, dims),
        mesh=mesh,
        in_specs=in_specs,
        out_specs=out_specs,
        check_vma=False,
    )
```

time: 270 us -> 41.4 us (0.15)
  waiting for transfers between devices: 130 us -> 0 us
  blocking collectives: 102 us -> 0 us
  Pallas kernels: 0 us -> 36 us
  between operations: 13.6 us -> 0.01 us
  matrix products: 11.9 us -> 0 us
  other arithmetic: 4.21 us -> 0 us
  local copies, waits for them, and re-layouts: 8.44 us -> 5.16 us
    unnamed x4 -> x0, waiting for transfers between devices: 130 us -> none
    all_gather x5 -> x0, blocking collectives: 81.4 us -> none  [the longest x1 42.2 us: local(): lax.all_gather(hidden[None], ('dp', 'kv', 'tp'), axis=0, tiled=True)]
    pallas_call x0 -> x1, Pallas kernels: none -> 36 us  [local(): pl.pallas_call(functools.partial(kernel, dims), name='layer', out_shape=j...]
    psum x1 -> x0, blocking collectives: 20.6 us -> none  [local(): lax.psum((part_q, part_k, part_v, local_sq), 'kv')]
    dot_general x8 -> x0, matrix products: 11.9 us -> none  [the longest x1 4.87 us: local(): jnp.einsum('arf,fcd->acrd', act, w_down.reshape(w_down.shape[0], blocks,...]
    unnamed x22 -> x1, local copies, waits for them, and re-layouts: 6.33 us -> 1.27 us
    reshape x3, local copies, waits for them, and re-layouts: 0.99 us -> 3.89 us  [the longest x1 1.31 us: local(): lam.reshape(-1, 1)]
  transfers between devices with their start and end apart: 2 -> 0, of which waited for: 2 -> 0; matrix products, arithmetic and copies ran while one was open for 0% -> 0% of each run, Pallas kernels for 0% -> 0%
where the time goes in v1:
time: 41.4 us; the launch traced here: 41.2 us
  Pallas kernels  36 us (87%)
  local copies, waits for them, and re-layouts  5.16 us (12%)
    pallas_call x1, Pallas kernels, local(): pl.pallas_call(functools.partial(kernel, dims), name='layer', out_shape=j...  36 us
    reshape x1, local copies, waits for them, and re-layouts, local(): lam.reshape(-1, 1)  1.31 us
    reshape x1, local copies, waits for them, and re-layouts, local(): ffn_gain.reshape(1, -1)  1.3 us
    reshape x1, local copies, waits for them, and re-layouts, local(): attn_gain.reshape(1, -1)  1.28 us
    unnamed x1, local copies, waits for them, and re-layouts  1.27 us

profile of v1, /device:TPU:0, one launch (start us, length us, event | category | flops | bytes accessed | tf_op | source)
XLA Modules:
  0.0 41.2 jit_solution(9176847109578456692)
XLA Ops:
  0.0 1.3 %reshape.18.gain = bf16[1,1024]{1,0:T(2,128)(2,1)} reshape(bf16[1024]{0:T(1024)(128)(2,1)} %param.15) | data formatting | bytes 4096 | tf_op jit(solution)/shard_map/reshape | solution.py:430
  1.3 1.3 %copy.15.lam = f32[8,1]{1,0:T(8,128)} copy(f32[8,1]{0,1:T(1,128)} %bitcast.7) | data formatting | bytes 64 | tf_op jit(solution)/shard_map/reshape | solution.py:431
  2.6 1.3 %reshape.21.ffn_gain = bf16[1,4096]{1,0:T(2,128)(2,1)} reshape(bf16[4096]{0:T(1024)(128)(2,1)} %param.24) | data formatting | bytes 16384 | tf_op jit(solution)/shard_map/reshape | solution.py:433
  3.9 36.0 %layer.1 = bf16[4,512]{1,0:T(4,128)(2,1)} custom-call(bf16[4,512]{1,0:T(4,128)(2,1)} %tok.1, bf16[1,1024]{1,0:T(2,128)(2,1)} %reshape.18.gain, f32[8,1]{1,0:T(8,128)} %copy.15.lam, bf16[1,128]{1,0:T(2,128)(2,1)} %bitcast.6, bf16[1,4096]{1,0:T(2,128)(2,1)} %reshape.21.ffn_gain, f32[2,128]{1,0:T(2,128)} %constant.2.clone.table, bf16[1024,1024]{1,0:T(8,128)(2,1)} %wq.1, ...), custom_call_target="tpu_custom_call" | custom-call | tf_op jit(solution)/shard_map/layer/pallas_call | solution.py:395
  39.9 1.3 %copy.17 = bf16[4,512]{1,0:T(4,128)(2,1)} copy(bf16[4,512]{1,0:T(4,128)(2,1)} %layer.1) | data formatting | bytes 8192

commit v2 on v1

--- a/solution.py
+++ b/solution.py
@@ -73,6 +73,7 @@
     half_in,
     hid,
     grid,
+    gains_two,
     down_out,
     down_in,
     load_sem,
@@ -88,7 +89,7 @@
     n = n_dp * n_kv * n_tp
     blocks = n_kv * n_tp
     rows, width = tok.shape
-    heads = lam.shape[0]
+    heads = lam.shape[1]
     q_cols = heads * VD
     model = blocks * width
     scale = HD ** (-0.5)
@@ -97,6 +98,12 @@
 
     def device(p):
         return (p // blocks, (p // n_tp) % n_kv, p % n_tp)
+
+    def gain_row(ref, c):
+        step = width // VD
+        return jnp.concatenate(
+            [ref[c * step + j : c * step + j + 1, :].astype(F32) for j in range(step)], axis=1
+        )
 
     loads = [
         pltpu.make_async_copy(src, dst, load_sem.at[k])
@@ -125,6 +132,26 @@
         return carry
 
     lax.fori_loop(1, n, greet, 0)
+
+    gains = [gain_row(gain, t) for t in range(n_tp)]
+
+    def project(t, value):
+        value = value.astype(F32)
+        row = gains[0]
+        for k in range(1, n_tp):
+            row = jnp.where(t == k, gains[k], row)
+        span = pl.ds(pl.multiple_of(t * width, width), width)
+        scaled = (value * row).astype(BF)
+        return (
+            jnp.dot(scaled, wq_v[span, :], preferred_element_type=F32),
+            jnp.dot(scaled, wk_v[span, :], preferred_element_type=F32),
+            jnp.dot(scaled, wv_v[span, :], preferred_element_type=F32),
+            jnp.sum(value * value, axis=-1, keepdims=True),
+        )
+
+    for load in loads[:3]:
+        load.wait()
+    sums = project(i_tp, tok[...])
     pl.semaphore_wait(barrier, n - 1)
 
     def to_tp(i, src, dst, sem):
@@ -171,8 +198,7 @@
             device_id_type=MESH,
         )
 
-    def to_all(i, src, dst, sem):
-        peer = (me + i) % n
+    def to_one(peer, src, dst, sem):
         return pltpu.make_async_remote_copy(
             src_ref=src(peer),
             dst_ref=dst.at[me],
@@ -182,16 +208,18 @@
             device_id_type=MESH,
         )
 
-    def from_all(i, dst, sem):
-        peer = (me + i) % n
-        return pltpu.make_async_remote_copy(
+    def to_all(i, src, dst, sem):
+        return to_one((me + i) % n, src, dst, sem)
+
+    def arrived(peer, dst, sem):
+        pltpu.make_async_remote_copy(
             src_ref=dst.at[peer],
             dst_ref=dst.at[peer],
             send_sem=sem.at[0, peer],
             recv_sem=sem.at[1, peer],
             device_id=device(peer),
             device_id_type=MESH,
-        )
+        ).wait_recv()
 
     def each(count, act):
         def step(i, carry):
@@ -202,35 +230,29 @@
 
     for i in range(1, n_tp):
         to_tp(i, lambda peer: tok, slab, slab_sem).start()
-    slab[i_tp] = tok[...]
-    for load in loads[:3]:
-        load.wait()
     for i in range(1, n_tp):
         from_tp(i, slab, slab_sem).wait_recv()
-
-    part_q = jnp.zeros((rows, q_cols), F32)
-    part_k = jnp.zeros((rows, VD), F32)
-    part_v = jnp.zeros((rows, VD), F32)
-    local_sq = jnp.zeros((rows, 1), F32)
-    for t in range(n_tp):
-        span = slice(t * width, (t + 1) * width)
-        value = slab[t].astype(F32)
-        local_sq += jnp.sum(value * value, axis=-1, keepdims=True)
-        scaled = (value * gain[:, span].astype(F32)).astype(BF)
-        part_q += jnp.dot(scaled, wq_v[span, :], preferred_element_type=F32)
-        part_k += jnp.dot(scaled, wk_v[span, :], preferred_element_type=F32)
-        part_v += jnp.dot(scaled, wv_v[span, :], preferred_element_type=F32)
-    part[i_kv, :, 0:q_cols] = part_q
-    part[i_kv, :, q_cols : q_cols + VD] = part_k
-    part[i_kv, :, q_cols + VD : q_cols + 2 * VD] = part_v
-    part[i_kv, :, q_cols + 2 * VD : q_cols + 3 * VD] = jnp.broadcast_to(local_sq, (rows, VD))
+        peer = (i_tp + i) % n_tp
+        sums = tuple(x + y for x, y in zip(sums, project(peer, slab[peer])))
+    part_q, part_k, part_v, local_sq = sums
+    part[i_kv, :, 0:q_cols] = part_q.astype(BF)
+    part[i_kv, :, q_cols : q_cols + VD] = part_k.astype(BF)
+    part[i_kv, :, q_cols + VD : q_cols + 2 * VD] = part_v.astype(BF)
+    lane_s = lax.broadcasted_iota(jnp.int32, (rows, VD), 1)
+    square = jnp.broadcast_to(local_sq, (rows, VD))
+    high = square.astype(BF).astype(F32)
+    middle = (square - high).astype(BF).astype(F32)
+    low = square - high - middle
+    terms = jnp.where(lane_s == 0, high, jnp.where(lane_s == 1, middle, low))
+    part[i_kv, :, q_cols + 2 * VD :] = jnp.where(lane_s < 3, terms, 0.0).astype(BF)
     each(n_kv, lambda i: to_kv(i, part, part_sem).start())
     each(n_kv, lambda i: from_kv(i, part, part_sem).wait_recv())
 
-    total = part[0]
+    total = part[0].astype(F32)
     for k in range(1, n_kv):
-        total += part[k]
-    inv_rms = lax.rsqrt(total[:, q_cols + 2 * VD : q_cols + 2 * VD + 1] / model + EPS)
+        total += part[k].astype(F32)
+    total_sq = jnp.sum(total[:, q_cols + 2 * VD :], axis=-1, keepdims=True)
+    inv_rms = lax.rsqrt(total_sq / model + EPS)
     table_v = table[...]
     for h in range(heads):
         chunk = total[:, h * VD : (h + 1) * VD] * inv_rms
@@ -267,18 +289,27 @@
         expo = jnp.exp(scores - top)
         den = jnp.sum(expo, axis=-1, keepdims=True)
         num = jnp.dot(expo.astype(BF), vc_v[r], preferred_element_type=F32)
-        o_part[i_kv, r] = (num / den).astype(BF)
+        o_part[r, i_kv] = (num / den).astype(BF)
+        for i in range(1, n_kv):
+            to_kv(i, o_part.at[r], o_sem.at[r]).start()
         stat = top + jnp.log(den)
         stat_row += jnp.sum(
             jnp.where(lane_p == row_p + r * pairs, stat, 0.0), axis=0, keepdims=True
         )
     s_part[i_kv] = jnp.broadcast_to(stat_row, (8, VD))
     each(n_kv, lambda i: to_kv(i, s_part, s_sem).start())
-    each(n_kv, lambda i: to_kv(i, o_part, o_sem).start())
     each(n_kv, lambda i: from_kv(i, s_part, s_sem).wait_recv())
-    each(n_kv, lambda i: from_kv(i, o_part, o_sem).wait_recv())
-
-    lam_h = lam[...]
+    for r in range(rows):
+        for i in range(1, n_kv):
+            from_kv(i, o_part.at[r], o_sem.at[r]).wait_recv()
+
+    head_row = lax.broadcasted_iota(jnp.int32, (heads, heads), 0)
+    head_lane = lax.broadcasted_iota(jnp.int32, (heads, heads), 1)
+    for c in range(blocks):
+        gains_two[c] = gain_row(ffn_gain, c)
+    lam_h = jnp.sum(
+        jnp.where(head_row == head_lane, lam[...], 0.0), axis=-1, keepdims=True
+    )
     for r in range(rows):
         own = own_scores[r]
         stats = []
@@ -297,7 +328,7 @@
         for k in range(n_kv):
             weight = jnp.exp(stats[k] - top)
             den += weight
-            num += weight * o_part[k, r].astype(F32)
+            num += weight * o_part[r, k].astype(F32)
         ratio = num / den
         mix = ratio[0:heads, :] - lam_h * ratio[heads:, :]
         normed = (
@@ -324,41 +355,68 @@
     hidden = (tok[...].astype(F32) + branch).astype(BF)
     hid[me] = hidden
     each(n, lambda i: to_all(i, lambda peer: hid.at[me], hid, hid_sem).start())
-    each(n, lambda i: from_all(i, hid, hid_sem).wait_recv())
-
+
+    order = sorted(range(n_kv), key=lambda j: min(j, n_kv - j))
     row_sq = jnp.zeros((n_dp * rows, 1), F32)
-    for c in range(blocks):
-        for a in range(n_dp):
-            grid[c, a * rows : (a + 1) * rows, :] = hid[a * blocks + c].astype(F32)
-        value = grid[c]
-        row_sq += jnp.sum(value * value, axis=-1, keepdims=True)
+    upward = jnp.zeros((n_dp * rows, wu_v.shape[1]), F32)
+    loads[6].wait()
+    for j in order:
+        for u in range(n_tp):
+            c = ((i_kv + j) % n_kv) * n_tp + (i_tp + u) % n_tp
+            for a in range(n_dp):
+                p = a * blocks + c
+                if j or u:
+                    arrived(p, hid, hid_sem)
+                else:
+
+                    @pl.when(p != me)
+                    def _():
+                        arrived(p, hid, hid_sem)
+
+                grid[c, a * rows : (a + 1) * rows, :] = hid[p].astype(F32)
+            value = grid[c]
+            row_sq += jnp.sum(value * value, axis=-1, keepdims=True)
+            span = pl.ds(pl.multiple_of(c * width, width), width)
+            upward += jnp.dot(
+                (value * gains_two[c]).astype(BF), wu_v[span, :], preferred_element_type=F32
+            )
     inv_two = lax.rsqrt(row_sq / model + EPS)
-    loads[6].wait()
-    upward = jnp.zeros((n_dp * rows, wu_v.shape[1]), F32)
-    for c in range(blocks):
-        span = slice(c * width, (c + 1) * width)
-        normed_two = (grid[c] * inv_two * ffn_gain[:, span].astype(F32)).astype(BF)
-        upward += jnp.dot(normed_two, wu_v[span, :], preferred_element_type=F32)
-    act = jnp.square(jnp.maximum(upward, 0.0)).astype(BF)
+    act = jnp.square(jnp.maximum(upward * inv_two, 0.0)).astype(BF)
     loads[7].wait()
-    for c in range(blocks):
-        span = slice(c * width, (c + 1) * width)
-        down = jnp.dot(act, wd_v[:, span], preferred_element_type=F32)
-        for a in range(n_dp):
-            down_out[a * blocks + c] = down[a * rows : (a + 1) * rows, :].astype(BF)
-    each(n, lambda i: to_all(i, lambda peer: down_out.at[peer], down_in, down_sem).start())
-    down_in[me] = down_out[me]
-    each(n, lambda i: from_all(i, down_in, down_sem).wait_recv())
-    mixed = down_in[0].astype(F32)
-    for p in range(1, n):
-        mixed += down_in[p].astype(F32)
+    for j in reversed(order):
+        for u in reversed(range(n_tp)):
+            c = ((i_kv + j) % n_kv) * n_tp + (i_tp + u) % n_tp
+            span = pl.ds(pl.multiple_of(c * width, width), width)
+            down = jnp.dot(act, wd_v[:, span], preferred_element_type=F32)
+            for a in range(n_dp):
+                down_out[a * blocks + c] = down[a * rows : (a + 1) * rows, :].astype(BF)
+            for a in reversed(range(n_dp)):
+                if j or u or a:
+                    to_one(
+                        ((i_dp + a) % n_dp) * blocks + c,
+                        lambda peer: down_out.at[peer],
+                        down_in,
+                        down_sem,
+                    ).start()
+    mixed = down_out[me].astype(F32)
+    for j in order:
+        for u in range(n_tp):
+            for a in range(n_dp):
+                if j or u or a:
+                    p = ((i_dp + a) % n_dp) * blocks
+                    p += ((i_kv + j) % n_kv) * n_tp + (i_tp + u) % n_tp
+                    arrived(p, down_in, down_sem)
+                    mixed += down_in[p].astype(F32)
     out[...] = (hidden.astype(F32) + mixed).astype(BF)
 
     for i in range(1, n_tp):
         to_tp(i, lambda peer: tok, slab, slab_sem).wait_send()
         to_tp(i, lambda peer: half_out.at[peer], half_in, half_sem).wait_send()
-    for dst, sem in ((part, part_sem), (s_part, s_sem), (o_part, o_sem)):
-        each(n_kv, lambda i: to_kv(i, dst, sem).wait_send())
+    each(n_kv, lambda i: to_kv(i, part, part_sem).wait_send())
+    each(n_kv, lambda i: to_kv(i, s_part, s_sem).wait_send())
+    for r in range(rows):
+        for i in range(1, n_kv):
+            to_kv(i, o_part.at[r], o_sem.at[r]).wait_send()
     each(n, lambda i: to_all(i, lambda peer: hid.at[me], hid, hid_sem).wait_send())
     each(n, lambda i: to_all(i, lambda peer: down_out.at[peer], down_in, down_sem).wait_send())
 
@@ -389,7 +447,7 @@
     values = value_cache.reshape(rows, positions, VD)
     table = jnp.asarray(rope_table(positions * n_kv))
     vmem = pl.BlockSpec(memory_space=pltpu.VMEM)
-    hbm = pl.BlockSpec(memory_space=pl.ANY)
+    hbm = pl.BlockSpec(memory_space=pltpu.HBM)
     big = (w_query, w_key, w_value, keys, values, w_out, w_up, w_down)
     dma = pltpu.SemaphoreType.DMA
     return pl.pallas_call(
@@ -401,36 +459,37 @@
         scratch_shapes=[pltpu.VMEM(a.shape, BF) for a in big]
         + [
             pltpu.VMEM((n_tp, rows, width), BF),
-            pltpu.VMEM((n_kv, rows, heads * VD + 3 * VD), F32),
+            pltpu.VMEM((n_kv, rows, heads * VD + 3 * VD), BF),
             pltpu.VMEM((rows, heads, VD), F32),
             pltpu.VMEM((8, VD), F32),
-            pltpu.VMEM((n_kv, rows, 2 * heads, VD), BF),
+            pltpu.VMEM((rows, n_kv, 2 * heads, VD), BF),
             pltpu.VMEM((n_kv, 8, VD), F32),
             pltpu.VMEM((rows, heads * VD), F32),
             pltpu.VMEM((n_tp, rows, width), BF),
             pltpu.VMEM((n_tp, rows, width), BF),
             pltpu.VMEM((n, rows, width), BF),
             pltpu.VMEM((blocks, n_dp * rows, width), F32),
+            pltpu.VMEM((blocks, 1, width), F32),
             pltpu.VMEM((n, rows, width), BF),
             pltpu.VMEM((n, rows, width), BF),
             dma((8,)),
             dma((2, n_tp)),
             dma((2, n_kv)),
-            dma((2, n_kv)),
+            dma((rows, 2, n_kv)),
             dma((2, n_kv)),
             dma((2, n_tp)),
             dma((2, n)),
             dma((2, n)),
         ],
         compiler_params=pltpu.CompilerParams(
-            collective_id=0, has_side_effects=True, vmem_limit_bytes=60 * 1024 * 1024
+            collective_id=0, has_side_effects=True, vmem_limit_bytes=63 * 1024 * 1024
         ),
     )(
         tokens,
-        attn_gain.reshape(1, -1),
-        lam.reshape(-1, 1),
+        attn_gain.reshape(-1, VD),
+        lam.reshape(1, -1),
         head_gain.reshape(1, -1),
-        ffn_gain.reshape(1, -1),
+        ffn_gain.reshape(-1, VD),
         table,
         *big,
     )

time: 41.4 us -> 37.6 us (0.908)
  local copies, waits for them, and re-layouts: 5.16 us -> 1.28 us
    reshape x3 -> x0, local copies, waits for them, and re-layouts: 3.89 us -> none  [the longest x1 1.31 us: local(): lam.reshape(-1, 1)]
where the time goes in v2:
time: 37.6 us; the launch traced here: 37.4 us
  Pallas kernels  36.1 us (96%)
  local copies, waits for them, and re-layouts  1.28 us (3%)
    pallas_call x1, Pallas kernels, local(): pl.pallas_call(functools.partial(kernel, dims), name='layer', out_shape=j...  36.1 us
    unnamed x1, local copies, waits for them, and re-layouts  1.28 us

profile of v2, /device:TPU:0, one launch (start us, length us, event | category | flops | bytes accessed | tf_op | source)
XLA Modules:
  0.0 37.4 jit_solution(15675172786297800121)
XLA Ops:
  0.0 36.1 %layer.1 = bf16[4,512]{1,0:T(4,128)(2,1)} custom-call(bf16[4,512]{1,0:T(4,128)(2,1)} %tok.1, bf16[8,128]{1,0:T(8,128)(2,1)} %bitcast.9, f32[1,8]{1,0:T(1,128)} %bitcast.10, bf16[1,128]{1,0:T(2,128)(2,1)} %bitcast.11, bf16[32,128]{1,0:T(8,128)(2,1)} %bitcast.8, f32[2,128]{1,0:T(2,128)} %constant.2.clone.table, bf16[1024,1024]{1,0:T(8,128)(2,1)} %wq.1, ...), custom_call_target="tpu_custom_call" | custom-call | tf_op jit(solution)/shard_map/layer/pallas_call | solution.py:453
  36.1 1.3 %copy.16 = bf16[4,512]{1,0:T(4,128)(2,1)} copy(bf16[4,512]{1,0:T(4,128)(2,1)} %layer.1) | data formatting | bytes 8192
